TPU v7x, 32 devices: a whole 2x2x4 slice. The times are simulated.
32 devices in a mesh: ep: 8 (over z, x), tp: 4 (over y, core).
Axes of the slice: x: 2, y: 2, z: 4, core: 2. Of those that a mesh axis runs over, the one named last changes fastest.
Arguments:
- tokens: bfloat16 [256, 2048], P('ep'), may hold values from -6 to 6
- state: float32 [256, 16, 128, 128], P('ep', 'tp'), may hold values from -6 to 6
- norm_gain: float32 [2048], replicated, may hold values from 0.1 to 1.9
- w_query: bfloat16 [2048, 2048], P(None, 'tp'), may hold values from -0.125 to 0.125
- w_forget: bfloat16 [2048, 2048], P(None, 'tp'), may hold values from -0.125 to 0.125
- w_input: bfloat16 [2048, 2048], P(None, 'tp'), may hold values from -0.125 to 0.125
- w_outgate: bfloat16 [2048, 2048], P(None, 'tp'), may hold values from -0.125 to 0.125
- forget_floor: float32 [2048], P('tp'), may hold values from 0.05 to 0.95
- head_gain: float32 [128], replicated, may hold values from 0.1 to 1.9
- w_out: bfloat16 [2048, 2048], P('tp'), may hold values from -0.125 to 0.125
- ffn_gain: float32 [2048], replicated, may hold values from 0.1 to 1.9
- routes: int32 [256, 2], P('ep'), may hold values from 0 to 7, all different within a row; in each aligned block of 32 rows (0 to 31, 32 to 63, ...) at most 16 rows name the same one
- route_weights: float32 [256, 2], P('ep'), may hold values from 0.2 to 1
- expert_gate: bfloat16 [8, 2048, 5632], P('ep', None, 'tp'), may hold values from -0.125 to 0.125
- expert_up: bfloat16 [8, 2048, 5632], P('ep', None, 'tp'), may hold values from -0.125 to 0.125
- expert_down: bfloat16 [8, 5632, 2048], P('ep', 'tp'), may hold values from -0.078125 to 0.078125
- dense_gate: bfloat16 [2048, 5632], P(None, 'ep'), may hold values from -0.125 to 0.125
- dense_up: bfloat16 [2048, 5632], P(None, 'ep'), may hold values from -0.125 to 0.125
- dense_down: bfloat16 [5632, 2048], P('ep'), may hold values from -0.078125 to 0.078125
- dense_mix: float32 [2048], replicated, may hold values from -6 to 6
Outputs:
- mixed: bfloat16 [256, 2048], P('ep')
- new_state: float32 [256, 16, 128, 128], P('ep', 'tp')
Inputs may be any that keep to these rules, and one draw needn't show every extreme that they name: `routes`: each row names 2 different experts; the rows of one index of ep name no expert more than 16 times, a bound that some block reaches.
All inputs are finite; a program needn't handle non-finite values.
Results may differ from a plain program's by a relative error of at most 0.014.
Values may be sent and summed in bfloat16 or wider, within the bound.
A program may use at most 128 MiB of HBM per device.

v0:
```python
import jax
import jax.numpy as jnp
from jax import lax
from jax.sharding import PartitionSpec as P

EPS = 1e-06


def rms_norm(value, gain):
    return value * lax.rsqrt(jnp.mean(value * value, axis=-1, keepdims=True) + EPS) * gain


def make_table(local_routes, experts, capacity):
    flat = local_routes.reshape(-1)
    onehot = (flat[:, None] == jnp.arange(experts, dtype=jnp.int32)[None, :]).astype(jnp.int32)
    before = jnp.cumsum(onehot, axis=0) - onehot
    slot = jnp.sum(before * onehot, axis=1)
    where = flat * capacity + slot
    return (where[:, None] == jnp.arange(experts * capacity, dtype=jnp.int32)[None, :]).astype(
        jnp.bfloat16
    )


def local(
    tokens,
    state,
    norm_gain,
    w_query,
    w_forget,
    w_input,
    w_outgate,
    forget_floor,
    head_gain,
    w_out,
    ffn_gain,
    routes,
    route_weights,
    expert_gate,
    expert_up,
    expert_down,
    dense_gate,
    dense_up,
    dense_down,
    dense_mix,
):
    seqs, width = tokens.shape
    local_heads = state.shape[1]
    key_size = state.shape[2]
    value_size = state.shape[3]
    resid_in = tokens.astype(jnp.float32)
    normed = rms_norm(resid_in, norm_gain).astype(jnp.bfloat16)
    zq = jnp.dot(normed, w_query, preferred_element_type=jnp.float32)
    zf = jnp.dot(normed, w_forget, preferred_element_type=jnp.float32)
    zi = jnp.dot(normed, w_input, preferred_element_type=jnp.float32)
    zg = jnp.dot(normed, w_outgate, preferred_element_type=jnp.float32)
    logf = jnp.logaddexp(jax.nn.log_sigmoid(zf), jnp.log(forget_floor) + jax.nn.log_sigmoid(-zf))
    logf = logf.reshape(seqs, local_heads, key_size)
    query = jax.nn.silu(zq).reshape(seqs, local_heads, key_size)
    keep = jnp.exp(logf)
    write = -jnp.expm1(logf)
    values = zi.reshape(seqs, local_heads, value_size)
    new_state = keep[..., None] * state + write[..., None] * values[:, :, None, :]
    read = jnp.einsum("thk,thkv->thv", query, new_state, precision=lax.Precision.HIGHEST)
    read = rms_norm(read, head_gain).reshape(seqs, local_heads * value_size)
    headout = (read * jax.nn.silu(zg)).astype(jnp.bfloat16)
    block_term = jnp.dot(headout, w_out, preferred_element_type=jnp.float32)
    block_term = block_term.astype(jnp.bfloat16).astype(jnp.float32)
    mixout = lax.psum(block_term.astype(jnp.bfloat16), "tp").astype(jnp.float32)
    resid = resid_in + mixout
    ffn_in = rms_norm(resid, ffn_gain).astype(jnp.bfloat16)
    piece = lax.all_gather(ffn_in, "ep", axis=0, tiled=True)
    dgate = jnp.dot(piece, dense_gate, preferred_element_type=jnp.float32)
    dupper = jnp.dot(piece, dense_up, preferred_element_type=jnp.float32)
    dense_hidden = (jax.nn.silu(dgate) * dupper).astype(jnp.bfloat16)
    rows = dense_hidden
    summed = lax.psum_scatter(
        jnp.dot(rows, dense_down, preferred_element_type=jnp.float32).astype(jnp.bfloat16),
        "ep",
        scatter_dimension=0,
        tiled=True,
    )
    dense = summed.astype(jnp.float32)
    experts = lax.axis_size("ep") * expert_gate.shape[0]
    top = routes.shape[1]
    capacity = 2 * seqs * top // experts
    table = make_table(routes, experts, capacity)
    repeated = jnp.repeat(ffn_in, top, axis=0)
    sent = jnp.dot(table.T, repeated, preferred_element_type=jnp.float32).astype(jnp.bfloat16)
    sent = sent.reshape(experts, capacity, width)
    arrived = lax.all_to_all(sent, "ep", split_axis=0, concat_axis=0, tiled=True)
    sources, items, _ = arrived.shape
    rows = arrived.reshape(sources * items, width)
    gate = jnp.dot(rows, expert_gate[0], preferred_element_type=jnp.float32)
    upper = jnp.dot(rows, expert_up[0], preferred_element_type=jnp.float32)
    hidden = (jax.nn.silu(gate) * upper).astype(jnp.bfloat16)
    part = jnp.dot(hidden, expert_down[0], preferred_element_type=jnp.float32)
    part = part.astype(jnp.bfloat16).astype(jnp.float32)
    summed_parts = lax.psum(part.astype(jnp.bfloat16), "tp")
    results = summed_parts.reshape(sources, items, width)
    back = lax.all_to_all(results, "ep", split_axis=0, concat_axis=0, tiled=True)
    picked = jnp.dot(
        table, back.reshape(experts * capacity, width), preferred_element_type=jnp.float32
    )
    weighted = picked * route_weights.reshape(seqs * top)[:, None]
    moe = jnp.sum(weighted.reshape(seqs, top, width), axis=1)
    mixed = (resid + moe + jax.nn.sigmoid(dense_mix) * dense).astype(jnp.bfloat16)
    return (mixed, new_state)


def solution(mesh):
    in_specs = (
        P("ep", None),
        P("ep", "tp", None, None),
        P(),
        P(None, "tp"),
        P(None, "tp"),
        P(None, "tp"),
        P(None, "tp"),
        P("tp"),
        P(),
        P("tp", None),
        P(),
        P("ep", None),
        P("ep", None),
        P("ep", None, "tp"),
        P("ep", None, "tp"),
        P("ep", "tp", None),
        P(None, "ep"),
        P(None, "ep"),
        P("ep", None),
        P(),
    )
    out_specs = (P("ep", None), P("ep", "tp", None, None))
    return jax.shard_map(local, mesh=mesh, in_specs=in_specs, out_specs=out_specs, check_vma=False)
```

profile of v0, /device:TPU:0, one launch (start us, length us, event | category | flops | bytes accessed | tf_op | source)
XLA Modules:
  0.0 235.8 jit_solution(614285579938243527)
XLA Ops:
  7.3 1.2 fusion.20
  8.5 2.2 divide_multiply_fusion
  10.7 2.2 fusion.38
  13.0 2.3 fusion.35
  15.3 8.2 %multiply_add_fusion = f32[32,4,128,128]{3,2,1,0:T(8,128)S(1)} fusion(f32[32,4,128,128]{3,2,1,0:T(8,128)} %param.21, f32[32,4,128]{2,1,0:T(4,128)S(1)} %mul.144, f32[32,4,128]{2,1,0:T(4,128)S(1)} %neg.60, f32[32,4,128]{2,1,0:T(4,128)S(1)} %exp.44), kind=kLoop, calls=%fused_computation | loop fusion | flops 6291456 | bytes 16973824 | tf_op jit(solution)/shard_map/add | solution.py:62
  23.6 7.3 %fusion.50 = f32[32,4,1,128]{3,2,1,0:T(1,128)S(1)} fusion(f32[32,4,128,1]{2,3,1,0:T(1,128)S(1)} %bitcast.52, f32[32,4,128,128]{3,2,1,0:T(8,128)S(1)} %multiply_add_fusion), kind=kOutput, calls=%fused_computation.59 | convolution fusion | flops 25165824 | bytes 8519680 | tf_op jit(solution)/shard_map/thk,thkv->thv/dot_general | solution.py:63
  31.1 3.8 %convolution_convert_fusion.2 = bf16[32,2048]{1,0:T(8,128)(2,1)} fusion(bf16[512,2048]{1,0:T(8,128)(2,1)} %param.29, f32[4,8,4,128]{3,2,1,0:T(4,128)S(1)} %bitcast.53, bf16[2048,512]{1,0:T(8,128)(2,1)} %param.26, bf16[32,2048]{1,0:T(8,128)(2,1)S(1)} %copy-done.2, f32[2048]{0:T(1024)S(1)} %copy-done.4, f32[32]{0:T(128)S(1)} %add_rsqrt_fusion.2), kind=kOutput, calls=%fused_computation.13 | convolution fusion | flops 134643712 | bytes 4530304 | tf_op jit(solution)/shard_map/dot_general | solution.py:66
  35.5 34.1 %all-reduce.3.cloned.1.call-done = bf16[32,2048]{1,0:T(8,128)(2,1)} async-done(((bf16[32,2048]{1,0:T(8,128)(2,1)}), bf16[32,2048]{1,0:T(8,128)(2,1)}) %all-reduce.3.cloned.1.call-update) | async-done | bytes 131088 | tf_op jit(solution)/shard_map/psum | solution.py:68
  72.6 2.1 convolution_convert_fusion.1
  74.8 5.5 %all-to-all-start = ((bf16[8,16,2048]{2,1,0:T(8,128)(2,1)}), bf16[8,16,2048]{2,1,0:T(8,128)(2,1)S(1)}, u32[]{:S(2)}, u32[]{:S(2)}) async-start(bf16[8,16,2048]{2,1,0:T(8,128)(2,1)} %bitcast.3), calls=%async_computation | async-start | bytes 1048576 | tf_op jit(solution)/shard_map/all_to_all | solution.py:90
  81.3 12.4 %all-to-all-done = bf16[8,16,2048]{2,1,0:T(8,128)(2,1)S(1)} async-done(((bf16[8,16,2048]{2,1,0:T(8,128)(2,1)}), bf16[8,16,2048]{2,1,0:T(8,128)(2,1)S(1)}, u32[]{:S(2)}, u32[]{:S(2)}) %all-to-all-start) | async-done | bytes 524320 | tf_op jit(solution)/shard_map/all_to_all | solution.py:90
  93.7 4.5 %fusion.4 = f32[128,1408]{1,0:T(8,128)} fusion(bf16[128,2048]{1,0:T(8,128)(2,1)S(1)} %bitcast.47, bf16[1,2048,1408]{2,1,0:T(8,128)(2,1)} %param.33), kind=kOutput, calls=%fused_computation.5 | convolution fusion | flops 738197504 | bytes 7012352 | tf_op jit(solution)/shard_map/dot_general | solution.py:93
  98.2 7.3 %fusion.12 = bf16[128,2048]{1,0:T(8,128)(2,1)} fusion(bf16[1,1408,2048]{2,1,0:T(8,128)(2,1)} %param.35, bf16[128,2048]{1,0:T(8,128)(2,1)S(1)} %bitcast.48, bf16[1,2048,1408]{2,1,0:T(8,128)(2,1)} %param.34, f32[128,1408]{1,0:T(8,128)} %fusion.4), kind=kOutput, calls=%fused_computation.11 | convolution fusion | flops 1477738496 | bytes 13303808 | tf_op jit(solution)/shard_map/dot_general | solution.py:96
  105.6 19.0 %all-gather.2.cloned.1.call-done = bf16[256,2048]{1,0:T(8,128)(2,1)} async-done(((bf16[32,2048]{1,0:T(8,128)(2,1)}), bf16[256,2048]{1,0:T(8,128)(2,1)}) %all-gather.2.cloned.1.call-update) | async-done | bytes 1048592 | tf_op jit(solution)/shard_map/all_gather | solution.py:71
  124.6 4.0 %fusion.51 = f32[256,704]{0,1:T(8,128)} fusion(bf16[256,2048]{1,0:T(8,128)(2,1)} %all-gather.2.cloned.1.call-done, bf16[2048,704]{0,1:T(8,128)(2,1)} %param.36), kind=kOutput, calls=%fused_computation.60 | convolution fusion | flops 738197504 | bytes 4653056 | tf_op jit(solution)/shard_map/dot_general | solution.py:72
  128.6 6.6 %convolution_convert_fusion = bf16[256,2048]{1,0:T(8,128)(2,1)} fusion(bf16[704,2048]{1,0:T(8,128)(2,1)S(1)} %copy-done, bf16[256,2048]{1,0:T(8,128)(2,1)} %all-gather.2.cloned.1.call-done, bf16[2048,704]{0,1:T(8,128)(2,1)} %param.37, f32[256,704]{0,1:T(8,128)} %fusion.51), kind=kOutput, calls=%fused_computation.7 | convolution fusion | flops 1478000640 | bytes 8585216 | tf_op jit(solution)/shard_map/dot_general | solution.py:77
  135.2 23.9 %all-reduce.5.cloned.1.call-done = bf16[8,16,2048]{2,1,0:T(8,128)(2,1)} async-done(((bf16[8,16,2048]{2,1,0:T(8,128)(2,1)}), bf16[8,16,2048]{2,1,0:T(8,128)(2,1)}) %all-reduce.5.cloned.1.call-update) | async-done | bytes 524304 | tf_op jit(solution)/shard_map/psum | solution.py:98
  159.1 5.5 %all-to-all-start.1 = ((bf16[8,16,2048]{2,1,0:T(8,128)(2,1)}), bf16[8,16,2048]{2,1,0:T(8,128)(2,1)S(1)}, u32[]{:S(2)}, u32[]{:S(2)}) async-start(bf16[8,16,2048]{2,1,0:T(8,128)(2,1)} %all-reduce.5.cloned.1.call-done), calls=%async_computation.1 | async-start | bytes 1048576 | tf_op jit(solution)/shard_map/all_to_all | solution.py:100
  166.7 15.4 %all-to-all-done.1 = bf16[8,16,2048]{2,1,0:T(8,128)(2,1)S(1)} async-done(((bf16[8,16,2048]{2,1,0:T(8,128)(2,1)}), bf16[8,16,2048]{2,1,0:T(8,128)(2,1)S(1)}, u32[]{:S(2)}, u32[]{:S(2)}) %all-to-all-start.1) | async-done | bytes 524320 | tf_op jit(solution)/shard_map/all_to_all | solution.py:100
  182.1 1.8 convolution_multiply_fusion
  183.8 1.4 reshape.94
  185.2 1.3 reduce_sum.49
  186.5 40.9 %reduce-scatter.2.cloned.1.call-done = bf16[32,2048]{1,0:T(8,128)(2,1)} async-done(((bf16[256,2048]{1,0:T(8,128)(2,1)}), bf16[32,2048]{1,0:T(8,128)(2,1)}) %reduce-scatter.2.cloned.1.call-update) | async-done | bytes 131088 | tf_op jit(solution)/shard_map/reduce_scatter | solution.py:76
  227.5 1.8 add_convert_fusion
  (51 shorter events, 7.1 us)
Async XLA Ops:
  7.2 121.4 %copy-start = (bf16[704,2048]{1,0:T(8,128)(2,1)S(1)}, bf16[704,2048]{1,0:T(8,128)(2,1)}, u32[]{:S(2)}) copy-start(bf16[704,2048]{1,0:T(8,128)(2,1)} %param.38) | copy-start | bytes 8650756
  7.2 5.8 %copy-start.2 = (bf16[32,2048]{1,0:T(8,128)(2,1)S(1)}, bf16[32,2048]{1,0:T(8,128)(2,1)}, u32[]{:S(2)}) copy-start(bf16[32,2048]{1,0:T(8,128)(2,1)} %param.20) | copy-start | bytes 393220
  7.2 5.8 %copy-start.4 = (f32[2048]{0:T(1024)S(1)}, f32[2048]{0:T(1024)}, u32[]{:S(2)}) copy-start(f32[2048]{0:T(1024)} %param.22) | copy-start | bytes 24580
  7.2 5.7 %copy-start.7 = (f32[512]{0:T(512)S(1)}, f32[512]{0:T(512)}, u32[]{:S(2)}) copy-start(f32[512]{0:T(512)} %param.27) | copy-start | bytes 6148
  7.2 62.4 %all-reduce.3.cloned.1.call-start = ((), (), s32[]{:S(2)}) async-start(), calls=%async_computation.3 | async-start | bytes 262144 | tf_op jit(solution)/shard_map/psum | solution.py:68
  23.5 7.3 %copy-start.1 = (f32[32,4,128,128]{3,2,1,0:T(8,128)}, f32[32,4,128,128]{3,2,1,0:T(8,128)S(1)}, u32[]{:S(2)}) copy-start(f32[32,4,128,128]{3,2,1,0:T(8,128)S(1)} %multiply_add_fusion) | copy-start | bytes 25165828
  23.6 7.4 %copy-start.9 = (f32[128]{0:T(128)S(1)}, f32[128]{0:T(128)}, u32[]{:S(2)}) copy-start(f32[128]{0:T(128)} %param.28) | copy-start | bytes 1540
  30.8 4.1 %copy-start.8 = (s32[32,2]{0,1:T(2,128)S(1)}, s32[32,2]{0,1:T(2,128)}, u32[]{:S(2)}) copy-start(s32[32,2]{0,1:T(2,128)} %param.31) | copy-start | bytes 772
  30.8 39.9 %copy-start.5 = (f32[2048]{0:T(1024)S(1)}, f32[2048]{0:T(1024)}, u32[]{:S(2)}) copy-start(f32[2048]{0:T(1024)} %param.30) | copy-start | bytes 24580
  35.5 39.3 %copy-start.6 = (s32[64]{0:T(128)}, s32[64]{0:T(128)S(1)}, u32[]{:S(2)}) copy-start(s32[64]{0:T(128)S(1)} %multiply_add_fusion.1) | copy-start | bytes 772
  71.7 3.1 %copy-start.3 = (bf16[32,2048]{1,0:T(8,128)(2,1)}, bf16[32,2048]{1,0:T(8,128)(2,1)S(1)}, u32[]{:S(2)}) copy-start(bf16[32,2048]{1,0:T(8,128)(2,1)S(1)} %multiply_convert_fusion) | copy-start | bytes 393220
  74.8 18.9 %all-to-all-start = ((bf16[8,16,2048]{2,1,0:T(8,128)(2,1)}), bf16[8,16,2048]{2,1,0:T(8,128)(2,1)S(1)}, u32[]{:S(2)}, u32[]{:S(2)}) async-start(bf16[8,16,2048]{2,1,0:T(8,128)(2,1)} %bitcast.3), calls=%async_computation | async-start | bytes 1048576 | tf_op jit(solution)/shard_map/all_to_all | solution.py:90
  80.3 44.3 %all-gather.2.cloned.1.call-start = ((), (), s32[]{:S(2)}) async-start(), calls=%async_computation.5 | async-start | bytes 1179648 | tf_op jit(solution)/shard_map/all_gather | solution.py:71
  81.1 78.1 %all-reduce.5.cloned.1.call-start = ((), (), s32[]{:S(2)}) async-start(), calls=%async_computation.4 | async-start | bytes 1048576 | tf_op jit(solution)/shard_map/psum | solution.py:98
  105.5 121.9 %reduce-scatter.2.cloned.1.call-start = ((), (), s32[]{:S(2)}) async-start(), calls=%async_computation.6 | async-start | bytes 1179648 | tf_op jit(solution)/shard_map/reduce_scatter | solution.py:76
  159.1 23.0 %all-to-all-start.1 = ((bf16[8,16,2048]{2,1,0:T(8,128)(2,1)}), bf16[8,16,2048]{2,1,0:T(8,128)(2,1)S(1)}, u32[]{:S(2)}, u32[]{:S(2)}) async-start(bf16[8,16,2048]{2,1,0:T(8,128)(2,1)} %all-reduce.5.cloned.1.call-done), calls=%async_computation.1 | async-start | bytes 1048576 | tf_op jit(solution)/shard_map/all_to_all | solution.py:100
Sparse Core Ops, SparseCore 0:
  35.1 34.4 all-reduce.2
  83.8 40.7 all-gather.1
  127.0 32.1 all-reduce.4
  162.4 65.0 reduce-scatter.1
where the time goes:
time: 237 us; the launch traced here: 236 us
  waiting for transfers between devices  147 us (62%)
  matrix products  44 us (19%)
  other arithmetic  15.9 us (7%)
  between operations  14 us (6%)
  starting transfers between devices  11.4 us (5%)
  local copies, waits for them, and re-layouts  4.03 us (2%)
    reduce_scatter x1, waiting for transfers between devices, local(): lax.psum_scatter(jnp.dot(rows, dense_down, preferred_element_type=jnp.flo...  40.9 us
    psum x1, waiting for transfers between devices, local(): mixout = lax.psum(block_term.astype(jnp.bfloat16), 'tp').astype(jnp.float32)  34.1 us
    psum x1, waiting for transfers between devices, local(): summed_parts = lax.psum(part.astype(jnp.bfloat16), 'tp')  23.9 us
    all_gather x1, waiting for transfers between devices, local(): piece = lax.all_gather(ffn_in, 'ep', axis=0, tiled=True)  19 us
    all_to_all x1, waiting for transfers between devices, local(): lax.all_to_all(results, 'ep', split_axis=0, concat_axis=0, tiled=True)  15.4 us
    all_to_all x1, waiting for transfers between devices, local(): lax.all_to_all(sent, 'ep', split_axis=0, concat_axis=0, tiled=True)  12.4 us
    add x1, other arithmetic, local(): keep[..., None] * state + write[..., None] * values[:, :, None, :]  8.22 us
    dot_general x1, matrix products, local(): part = jnp.dot(hidden, expert_down[0], preferred_element_type=jnp.float32)  7.29 us
  transfers between devices with their start and end apart: 6, of which 6 were waited for; matrix products, arithmetic and copies ran while one was open for 12% of the time, Pallas kernels for 0%

commit v1 on v0

--- a/solution.py
+++ b/solution.py
@@ -95,7 +95,7 @@
     hidden = (jax.nn.silu(gate) * upper).astype(jnp.bfloat16)
     part = jnp.dot(hidden, expert_down[0], preferred_element_type=jnp.float32)
     part = part.astype(jnp.bfloat16).astype(jnp.float32)
-    summed_parts = lax.psum(part.astype(jnp.bfloat16), "tp")
+    summed_parts = jnp.sum(lax.all_gather(part.astype(jnp.bfloat16), "tp"), axis=0)
     results = summed_parts.reshape(sources, items, width)
     back = lax.all_to_all(results, "ep", split_axis=0, concat_axis=0, tiled=True)
     picked = jnp.dot(

time: 237 us -> 226 us (0.954)
  waiting for transfers between devices: 147 us -> 133 us
  other arithmetic: 15.9 us -> 18.8 us
    psum x1 -> x0, waiting for transfers between devices: 23.9 us -> none  [local(): summed_parts = lax.psum(part.astype(jnp.bfloat16), 'tp')]
    all_gather x0 -> x1, waiting for transfers between devices: none -> 12.3 us  [local(): lax.all_gather(part.astype(jnp.bfloat16), 'tp')]
    reduce_scatter x1, waiting for transfers between devices: 40.9 us -> 35.7 us  [local(): lax.psum_scatter(jnp.dot(rows, dense_down, preferred_element_type=jnp.flo...]
    all_to_all x1, waiting for transfers between devices: 15.4 us -> 18.8 us  [local(): lax.all_to_all(results, 'ep', split_axis=0, concat_axis=0, tiled=True)]
    reduce_sum x0 -> x1, other arithmetic: none -> 2.91 us  [local(): jnp.sum(lax.all_gather(part.astype(jnp.bfloat16), 'tp'), axis=0)]
  transfers between devices with their start and end apart: 6 -> 6, of which waited for: 6 -> 6; matrix products, arithmetic and copies ran while one was open for 12% -> 14% of each run, Pallas kernels for 0% -> 0%
where the time goes in v1:
time: 226 us; the launch traced here: 225 us
  waiting for transfers between devices  133 us (59%)
  matrix products  44 us (19%)
  other arithmetic  18.8 us (8%)
  between operations  14 us (6%)
  starting transfers between devices  11.4 us (5%)
  local copies, waits for them, and re-layouts  4.03 us (2%)
    reduce_scatter x1, waiting for transfers between devices, local(): lax.psum_scatter(jnp.dot(rows, dense_down, preferred_element_type=jnp.flo...  35.7 us
    psum x1, waiting for transfers between devices, local(): mixout = lax.psum(block_term.astype(jnp.bfloat16), 'tp').astype(jnp.float32)  34.1 us
    all_gather x1, waiting for transfers between devices, local(): piece = lax.all_gather(ffn_in, 'ep', axis=0, tiled=True)  19 us
    all_to_all x1, waiting for transfers between devices, local(): lax.all_to_all(results, 'ep', split_axis=0, concat_axis=0, tiled=True)  18.8 us
    all_to_all x1, waiting for transfers between devices, local(): lax.all_to_all(sent, 'ep', split_axis=0, concat_axis=0, tiled=True)  12.4 us
    all_gather x1, waiting for transfers between devices, local(): lax.all_gather(part.astype(jnp.bfloat16), 'tp')  12.3 us
    add x1, other arithmetic, local(): keep[..., None] * state + write[..., None] * values[:, :, None, :]  8.22 us
    dot_general x1, matrix products, local(): part = jnp.dot(hidden, expert_down[0], preferred_element_type=jnp.float32)  7.28 us
  transfers between devices with their start and end apart: 6, of which 6 were waited for; matrix products, arithmetic and copies ran while one was open for 14% of the time, Pallas kernels for 0%

profile of v1, /device:TPU:0, one launch (start us, length us, event | category | flops | bytes accessed | tf_op | source)
XLA Modules:
  0.0 225.2 jit_solution(4487370958331138882)
XLA Ops:
  8.5 2.2 divide_multiply_fusion
  10.7 2.2 fusion.38
  13.0 2.3 %fusion.35 = (f32[32,512]{1,0:T(8,128)S(1)}, f32[32,512]{1,0:T(8,128)S(1)}) fusion(f32[512]{0:T(512)S(1)} %log.3, bf16[2048,512]{1,0:T(8,128)(2,1)} %param.24, bf16[32,2048]{1,0:T(8,128)(2,1)S(1)} %copy-done.2, f32[2048]{0:T(1024)S(1)} %copy-done.4, f32[32]{0:T(128)S(1)} %add_rsqrt_fusion.2), kind=kOutput, calls=%fused_computation.54 | convolution fusion | flops 67780608 | bytes 2369664 | tf_op jit(solution)/shard_map/dot_general | solution.py:53
  15.3 8.2 %multiply_add_fusion = f32[32,4,128,128]{3,2,1,0:T(8,128)S(1)} fusion(f32[32,4,128,128]{3,2,1,0:T(8,128)} %param.21, f32[32,4,128]{2,1,0:T(4,128)S(1)} %mul.144, f32[32,4,128]{2,1,0:T(4,128)S(1)} %neg.60, f32[32,4,128]{2,1,0:T(4,128)S(1)} %exp.44), kind=kLoop, calls=%fused_computation | loop fusion | flops 6291456 | bytes 16973824 | tf_op jit(solution)/shard_map/add | solution.py:62
  23.6 7.3 %fusion.50 = f32[32,4,1,128]{3,2,1,0:T(1,128)S(1)} fusion(f32[32,4,128,1]{2,3,1,0:T(1,128)S(1)} %bitcast.54, f32[32,4,128,128]{3,2,1,0:T(8,128)S(1)} %multiply_add_fusion), kind=kOutput, calls=%fused_computation.59 | convolution fusion | flops 25165824 | bytes 8519680 | tf_op jit(solution)/shard_map/thk,thkv->thv/dot_general | solution.py:63
  31.1 3.8 %convolution_convert_fusion.2 = bf16[32,2048]{1,0:T(8,128)(2,1)} fusion(bf16[512,2048]{1,0:T(8,128)(2,1)} %param.29, f32[4,8,4,128]{3,2,1,0:T(4,128)S(1)} %bitcast.55, bf16[2048,512]{1,0:T(8,128)(2,1)} %param.26, bf16[32,2048]{1,0:T(8,128)(2,1)S(1)} %copy-done.2, f32[2048]{0:T(1024)S(1)} %copy-done.4, f32[32]{0:T(128)S(1)} %add_rsqrt_fusion.2), kind=kOutput, calls=%fused_computation.13 | convolution fusion | flops 134643712 | bytes 4530304 | tf_op jit(solution)/shard_map/dot_general | solution.py:66
  35.5 34.1 %all-reduce.2.cloned.1.call-done = bf16[32,2048]{1,0:T(8,128)(2,1)} async-done(((bf16[32,2048]{1,0:T(8,128)(2,1)}), bf16[32,2048]{1,0:T(8,128)(2,1)}) %all-reduce.2.cloned.1.call-update) | async-done | bytes 131088 | tf_op jit(solution)/shard_map/psum | solution.py:68
  72.6 2.1 convolution_convert_fusion.1
  74.8 5.5 %all-to-all-start = ((bf16[8,16,2048]{2,1,0:T(8,128)(2,1)}), bf16[8,16,2048]{2,1,0:T(8,128)(2,1)S(1)}, u32[]{:S(2)}, u32[]{:S(2)}) async-start(bf16[8,16,2048]{2,1,0:T(8,128)(2,1)} %bitcast.3), calls=%async_computation | async-start | bytes 1048576 | tf_op jit(solution)/shard_map/all_to_all | solution.py:90
  81.3 12.4 %all-to-all-done = bf16[8,16,2048]{2,1,0:T(8,128)(2,1)S(1)} async-done(((bf16[8,16,2048]{2,1,0:T(8,128)(2,1)}), bf16[8,16,2048]{2,1,0:T(8,128)(2,1)S(1)}, u32[]{:S(2)}, u32[]{:S(2)}) %all-to-all-start) | async-done | bytes 524320 | tf_op jit(solution)/shard_map/all_to_all | solution.py:90
  93.7 4.5 %fusion.4 = f32[128,1408]{1,0:T(8,128)} fusion(bf16[128,2048]{1,0:T(8,128)(2,1)S(1)} %bitcast.50, bf16[1,2048,1408]{2,1,0:T(8,128)(2,1)} %param.33), kind=kOutput, calls=%fused_computation.5 | convolution fusion | flops 738197504 | bytes 7012352 | tf_op jit(solution)/shard_map/dot_general | solution.py:93
  98.2 7.3 %fusion.12 = bf16[128,2048]{1,0:T(8,128)(2,1)} fusion(bf16[1,1408,2048]{2,1,0:T(8,128)(2,1)} %param.35, bf16[128,2048]{1,0:T(8,128)(2,1)S(1)} %bitcast.51, bf16[1,2048,1408]{2,1,0:T(8,128)(2,1)} %param.34, f32[128,1408]{1,0:T(8,128)} %fusion.4), kind=kOutput, calls=%fused_computation.11 | convolution fusion | flops 1477738496 | bytes 13303808 | tf_op jit(solution)/shard_map/dot_general | solution.py:96
  105.6 19.0 %all-gather.4.cloned.1.call-done = bf16[256,2048]{1,0:T(8,128)(2,1)} async-done(((bf16[32,2048]{1,0:T(8,128)(2,1)}), bf16[256,2048]{1,0:T(8,128)(2,1)}) %all-gather.4.cloned.1.call-update) | async-done | bytes 1048592 | tf_op jit(solution)/shard_map/all_gather | solution.py:71
  124.6 3.9 %fusion.51 = f32[256,704]{0,1:T(8,128)} fusion(bf16[256,2048]{1,0:T(8,128)(2,1)} %all-gather.4.cloned.1.call-done, bf16[2048,704]{0,1:T(8,128)(2,1)} %param.36), kind=kOutput, calls=%fused_computation.60 | convolution fusion | flops 738197504 | bytes 4653056 | tf_op jit(solution)/shard_map/dot_general | solution.py:72
  128.6 6.6 %convolution_convert_fusion = bf16[256,2048]{1,0:T(8,128)(2,1)} fusion(bf16[704,2048]{1,0:T(8,128)(2,1)S(1)} %copy-done, bf16[256,2048]{1,0:T(8,128)(2,1)} %all-gather.4.cloned.1.call-done, bf16[2048,704]{0,1:T(8,128)(2,1)} %param.37, f32[256,704]{0,1:T(8,128)} %fusion.51), kind=kOutput, calls=%fused_computation.7 | convolution fusion | flops 1478000640 | bytes 8585216 | tf_op jit(solution)/shard_map/dot_general | solution.py:77
  135.2 12.3 %all-gather.6.cloned.1.call-done = bf16[512,2048]{1,0:T(8,128)(2,1)} async-done(((bf16[128,2048]{1,0:T(8,128)(2,1)}), bf16[512,2048]{1,0:T(8,128)(2,1)}) %all-gather.6.cloned.1.call-update) | async-done | bytes 2097168 | tf_op jit(solution)/shard_map/all_gather | solution.py:98
  147.5 2.9 %reduce_sum.61 = bf16[128,2048]{1,0:T(8,128)(2,1)} reduce(bf16[4,128,2048]{2,1,0:T(8,128)(2,1)} %bitcast.48, bf16[]{:T(256)} %constant.34.clone.1), dimensions={0}, to_apply=%region_6.7 | reduce | flops 786432 | bytes 2621442 | tf_op jit(solution)/shard_map/reduce_sum | solution.py:98
  150.4 5.5 %all-to-all-start.1 = ((bf16[8,16,2048]{2,1,0:T(8,128)(2,1)}), bf16[8,16,2048]{2,1,0:T(8,128)(2,1)S(1)}, u32[]{:S(2)}, u32[]{:S(2)}) async-start(bf16[8,16,2048]{2,1,0:T(8,128)(2,1)} %bitcast.49), calls=%async_computation.1 | async-start | bytes 1048576 | tf_op jit(solution)/shard_map/all_to_all | solution.py:100
  158.0 18.8 %all-to-all-done.1 = bf16[8,16,2048]{2,1,0:T(8,128)(2,1)S(1)} async-done(((bf16[8,16,2048]{2,1,0:T(8,128)(2,1)}), bf16[8,16,2048]{2,1,0:T(8,128)(2,1)S(1)}, u32[]{:S(2)}, u32[]{:S(2)}) %all-to-all-start.1) | async-done | bytes 524320 | tf_op jit(solution)/shard_map/all_to_all | solution.py:100
  176.8 1.7 convolution_multiply_fusion
  178.5 1.4 reshape.94
  179.8 1.3 reduce_sum.62
  181.2 35.7 %reduce-scatter.2.cloned.1.call-done = bf16[32,2048]{1,0:T(8,128)(2,1)} async-done(((bf16[256,2048]{1,0:T(8,128)(2,1)}), bf16[32,2048]{1,0:T(8,128)(2,1)}) %reduce-scatter.2.cloned.1.call-update) | async-done | bytes 131088 | tf_op jit(solution)/shard_map/reduce_scatter | solution.py:76
  216.9 1.8 add_convert_fusion
  (52 shorter events, 8.3 us)
Async XLA Ops:
  7.2 121.4 %copy-start = (bf16[704,2048]{1,0:T(8,128)(2,1)S(1)}, bf16[704,2048]{1,0:T(8,128)(2,1)}, u32[]{:S(2)}) copy-start(bf16[704,2048]{1,0:T(8,128)(2,1)} %param.38) | copy-start | bytes 8650756
  7.2 5.8 %copy-start.2 = (bf16[32,2048]{1,0:T(8,128)(2,1)S(1)}, bf16[32,2048]{1,0:T(8,128)(2,1)}, u32[]{:S(2)}) copy-start(bf16[32,2048]{1,0:T(8,128)(2,1)} %param.20) | copy-start | bytes 393220
  7.2 5.8 %copy-start.4 = (f32[2048]{0:T(1024)S(1)}, f32[2048]{0:T(1024)}, u32[]{:S(2)}) copy-start(f32[2048]{0:T(1024)} %param.22) | copy-start | bytes 24580
  7.2 5.7 %copy-start.7 = (f32[512]{0:T(512)S(1)}, f32[512]{0:T(512)}, u32[]{:S(2)}) copy-start(f32[512]{0:T(512)} %param.27) | copy-start | bytes 6148
  7.2 62.4 %all-reduce.2.cloned.1.call-start = ((), (), s32[]{:S(2)}) async-start(), calls=%async_computation.3 | async-start | bytes 262144 | tf_op jit(solution)/shard_map/psum | solution.py:68
  23.5 7.3 %copy-start.1 = (f32[32,4,128,128]{3,2,1,0:T(8,128)}, f32[32,4,128,128]{3,2,1,0:T(8,128)S(1)}, u32[]{:S(2)}) copy-start(f32[32,4,128,128]{3,2,1,0:T(8,128)S(1)} %multiply_add_fusion) | copy-start | bytes 25165828
  23.6 7.4 %copy-start.9 = (f32[128]{0:T(128)S(1)}, f32[128]{0:T(128)}, u32[]{:S(2)}) copy-start(f32[128]{0:T(128)} %param.28) | copy-start | bytes 1540
  30.8 4.1 %copy-start.8 = (s32[32,2]{0,1:T(2,128)S(1)}, s32[32,2]{0,1:T(2,128)}, u32[]{:S(2)}) copy-start(s32[32,2]{0,1:T(2,128)} %param.31) | copy-start | bytes 772
  30.8 39.9 %copy-start.5 = (f32[2048]{0:T(1024)S(1)}, f32[2048]{0:T(1024)}, u32[]{:S(2)}) copy-start(f32[2048]{0:T(1024)} %param.30) | copy-start | bytes 24580
  35.5 39.3 %copy-start.6 = (s32[64]{0:T(128)}, s32[64]{0:T(128)S(1)}, u32[]{:S(2)}) copy-start(s32[64]{0:T(128)S(1)} %multiply_add_fusion.1) | copy-start | bytes 772
  71.7 3.1 %copy-start.3 = (bf16[32,2048]{1,0:T(8,128)(2,1)}, bf16[32,2048]{1,0:T(8,128)(2,1)S(1)}, u32[]{:S(2)}) copy-start(bf16[32,2048]{1,0:T(8,128)(2,1)S(1)} %multiply_convert_fusion) | copy-start | bytes 393220
  74.8 18.9 %all-to-all-start = ((bf16[8,16,2048]{2,1,0:T(8,128)(2,1)}), bf16[8,16,2048]{2,1,0:T(8,128)(2,1)S(1)}, u32[]{:S(2)}, u32[]{:S(2)}) async-start(bf16[8,16,2048]{2,1,0:T(8,128)(2,1)} %bitcast.3), calls=%async_computation | async-start | bytes 1048576 | tf_op jit(solution)/shard_map/all_to_all | solution.py:90
  80.3 44.3 %all-gather.4.cloned.1.call-start = ((), (), s32[]{:S(2)}) async-start(), calls=%async_computation.4 | async-start | bytes 1179648 | tf_op jit(solution)/shard_map/all_gather | solution.py:71
  81.1 66.4 %all-gather.6.cloned.1.call-start = ((), (), s32[]{:S(2)}) async-start(), calls=%async_computation.6 | async-start | bytes 2621440 | tf_op jit(solution)/shard_map/all_gather | solution.py:98
  105.5 111.4 %reduce-scatter.2.cloned.1.call-start = ((), (), s32[]{:S(2)}) async-start(), calls=%async_computation.5 | async-start | bytes 1179648 | tf_op jit(solution)/shard_map/reduce_scatter | solution.py:76
  150.4 26.4 %all-to-all-start.1 = ((bf16[8,16,2048]{2,1,0:T(8,128)(2,1)}), bf16[8,16,2048]{2,1,0:T(8,128)(2,1)S(1)}, u32[]{:S(2)}, u32[]{:S(2)}) async-start(bf16[8,16,2048]{2,1,0:T(8,128)(2,1)} %bitcast.49), calls=%async_computation.1 | async-start | bytes 1048576 | tf_op jit(solution)/shard_map/all_to_all | solution.py:100
Sparse Core Ops, SparseCore 0:
  35.1 34.4 all-reduce.1
  83.8 40.7 all-gather.3
  126.2 21.2 all-gather.5
  150.7 66.1 reduce-scatter.1
